TPU v7x, 32 devices: a whole 2x2x4 slice. The times are simulated.
32 devices in a mesh: sp: 4 (over z), fs: 4 (over y, x), tp: 2 (over core).
Axes of the slice: x: 2, y: 2, z: 4, core: 2. Of those that a mesh axis runs over, the one named last changes fastest.
Arguments:
- tokens: bfloat16 [1024, 2048], P('sp', ('fs', 'tp')), may hold values from -500 to 500
- norm_gain: float32 [2048], replicated, may hold values from 0.1 to 1.9
- query_w: bfloat16 [2048, 1024], P('sp', ('fs', 'tp')), may hold values from -1 to 1
- key_w: bfloat16 [2048, 512], P('sp', ('fs', 'tp')), may hold values from -1 to 1
- value_w: bfloat16 [2048, 512], P('sp', ('fs', 'tp')), may hold values from -0.125 to 0.125
- recept_w: bfloat16 [2048, 1024], P('sp', ('fs', 'tp')), may hold values from -0.125 to 0.125
- rec_key_w: bfloat16 [2048, 1024], P('sp', ('fs', 'tp')), may hold values from -0.125 to 0.125
- rec_value_w: bfloat16 [2048, 1024], P('sp', ('fs', 'tp')), may hold values from -0.125 to 0.125
- decay_down: bfloat16 [2048, 64], replicated, may hold values from -0.125 to 0.125
- decay_up: bfloat16 [64, 1024], replicated, may hold values from -1 to 1
- decay_base: float32 [16, 1024], P(('fs', 'tp'), 'sp'), may hold values from -14 to 0
- learn_rate: float32 [1024], P(('fs', 'tp')), may hold values from 0.1 to 1
- query_gain: float32 [64], replicated, may hold values from 0 to 7
- key_gain: float32 [64], replicated, may hold values from 0 to 7
- sink_logit: float32 [16], P(('fs', 'tp')), may hold values from 1 to 5
- group_gain: float32 [1024], P(('fs', 'tp')), may hold values from 0.1 to 1.9
- out_att_w: bfloat16 [1024, 2048], P(('fs', 'tp'), 'sp'), may hold values from -0.75 to 0.75
- out_rec_w: bfloat16 [1024, 2048], P(('fs', 'tp'), 'sp'), may hold values from -0.1875 to 0.1875
Outputs:
- mixed: bfloat16 [1024, 2048], P(('sp', 'fs', 'tp'))
- row_lse: float32 [16, 1024], P(('fs', 'tp'), 'sp')
All inputs are finite; a program needn't handle non-finite values.
Results may differ from a plain program's by a relative error of at most 0.015.
Values may be sent and summed in bfloat16 or wider, within the bound.
A program may use at most 64 MiB of HBM per device.

v0:
```python
import math
import jax
import jax.numpy as jnp
from jax import lax
from jax.sharding import PartitionSpec as P

HEAD = 64
WINDOW = 128
BLOCK = 32
NORM_EPS = 1e-06
KEY_EPS = 1e-06
GROUP_EPS = 0.00064
EXACT_PRECISION = lax.Precision.HIGHEST


def passed_along(array, axis, by):
    devices = lax.axis_size(axis)
    pairs = [(i, i + by) for i in range(devices) if 0 <= i + by < devices]
    return lax.ppermute(array, axis, pairs)


def prefix(array, axis, combine, identity):
    devices, place = (lax.axis_size(axis), lax.axis_index(axis))
    everything = lax.all_gather(array.astype(jnp.bfloat16), axis)
    start = jnp.broadcast_to(jnp.asarray(identity, array.dtype), array.shape)

    def turn(k, before):
        reached = k < place
        new = combine(before, everything[k].astype(array.dtype))
        return jnp.where(reached, new, before)

    return lax.fori_loop(0, devices, turn, start)


def head_rms(values, gain_vec, num_heads):
    shaped = values.astype(jnp.float32).reshape(values.shape[0], num_heads, HEAD)
    mean_sq = jnp.mean(shaped * shaped, axis=-1, keepdims=True)
    return (shaped * lax.rsqrt(mean_sq + NORM_EPS) * gain_vec).astype(jnp.bfloat16)


def attend(query_rows, key_rows, value_rows, query_gain, key_gain, sink_logit):
    num_rows = query_rows.shape[0]
    num_heads = query_rows.shape[1] // HEAD
    kv_heads = key_rows.shape[1] // HEAD
    group_size = num_heads // kv_heads
    blocks = num_rows // WINDOW
    query_n = head_rms(query_rows, query_gain, num_heads).reshape(
        blocks, WINDOW, kv_heads, group_size, HEAD
    )
    key_n = head_rms(key_rows, key_gain, kv_heads).reshape(num_rows, kv_heads * HEAD)
    paired = jnp.concatenate([key_n, value_rows], axis=1)
    before = passed_along(paired[num_rows - WINDOW :], "sp", 1)
    current = paired.reshape(blocks, WINDOW, 2 * kv_heads * HEAD)
    previous = jnp.concatenate([before[None], current[:-1]], axis=0)
    key_band = jnp.concatenate([previous, current], axis=1).reshape(
        blocks, 2 * WINDOW, 2, kv_heads, HEAD
    )
    scores = jnp.einsum(
        "nqkgd,nskd->nkgqs", query_n, key_band[:, :, 0], preferred_element_type=jnp.float32
    ) * (1.0 / math.sqrt(HEAD))
    offset = lax.axis_index("sp") * num_rows
    lag_table = (
        lax.broadcasted_iota(jnp.int32, (WINDOW, 2 * WINDOW), 0)
        + WINDOW
        - lax.broadcasted_iota(jnp.int32, (WINDOW, 2 * WINDOW), 1)
    )
    key_place = (
        offset
        + (lax.broadcasted_iota(jnp.int32, (blocks, 2 * WINDOW), 0) - 1) * WINDOW
        + lax.broadcasted_iota(jnp.int32, (blocks, 2 * WINDOW), 1)
    )
    allowed = ((lag_table >= 0) & (lag_table < WINDOW))[None, :, :] & (key_place >= 0)[:, None, :]
    allowed = allowed[:, None, None]
    sink_cols = sink_logit.reshape(kv_heads, group_size)[None, :, :, None, None]
    masked = jnp.where(allowed, scores, -jnp.inf)
    row_top = jnp.maximum(jnp.max(masked, axis=-1, keepdims=True), sink_cols)
    weight = jnp.where(allowed, jnp.exp(masked - row_top), 0.0)
    row_total = jnp.sum(weight, axis=-1, keepdims=True) + jnp.exp(sink_cols - row_top)
    row_lse = (
        (row_top + jnp.log(row_total))[..., 0].transpose(1, 2, 0, 3).reshape(num_heads, num_rows)
    )
    att_probs = (weight / row_total).astype(jnp.bfloat16)
    mixed_heads = jnp.einsum(
        "nkgqs,nskd->nqkgd", att_probs, key_band[:, :, 1], preferred_element_type=jnp.float32
    )
    return (mixed_heads.reshape(num_rows, num_heads * HEAD).astype(jnp.bfloat16), row_lse)


def unit_inverse(lower_mat):
    mat_size = lower_mat.shape[-1]
    result = jnp.eye(mat_size, dtype=jnp.float32) + lower_mat
    power_mat = lower_mat
    for section_index in range(mat_size.bit_length() - 2):
        power_mat = jnp.einsum("hij,hjk->hik", power_mat, power_mat, precision=EXACT_PRECISION)
        result = result + jnp.einsum("hij,hjk->hik", result, power_mat, precision=EXACT_PRECISION)
    return result


def pair_table(left_vals, right_vals, allowed):
    return jnp.where(
        allowed, jnp.einsum("hid,hjd->hij", left_vals, right_vals, precision=EXACT_PRECISION), 0.0
    )


def recur(reads, rec_keys, rec_values, log_decay, learn_rate, group_gain):
    num_rows = reads.shape[0]
    num_heads = reads.shape[1] // HEAD
    blocks = num_rows // BLOCK

    def by_block(values):
        return (
            values.astype(jnp.float32).reshape(blocks, BLOCK, num_heads, HEAD).transpose(0, 2, 1, 3)
        )

    read_vals = by_block(reads)
    key_vals = by_block(rec_keys)
    value_vals = by_block(rec_values)
    decay_vals = by_block(log_decay)
    unit_key = key_vals * lax.rsqrt(jnp.sum(key_vals * key_vals, axis=-1, keepdims=True) + KEY_EPS)
    removal = -unit_key
    writing = unit_key * learn_rate.reshape(num_heads, HEAD)[None, :, None, :]
    stacked = jnp.concatenate([jnp.zeros_like(value_vals), value_vals], axis=-1)
    unit_matrix = jnp.broadcast_to(jnp.eye(HEAD, dtype=jnp.float32), (num_heads, HEAD, HEAD))
    start_pair = jnp.concatenate(
        [unit_matrix, jnp.zeros((num_heads, HEAD, HEAD), jnp.float32)], axis=1
    )
    row_iota = lax.broadcasted_iota(jnp.int32, (BLOCK, BLOCK), 0)
    col_iota = lax.broadcasted_iota(jnp.int32, (BLOCK, BLOCK), 1)
    strict = (row_iota > col_iota)[None]
    inclusive = (row_iota >= col_iota)[None]

    def block_step(state_per_block, inputs):
        read_now, key_now, removal_now, writing_now, decay_now, current_value = inputs
        cum_decay = jnp.cumsum(decay_now, axis=1)
        decay_matrix_a = removal_now * jnp.exp(cum_decay - decay_now)
        decay_matrix_b = writing_now * jnp.exp(-cum_decay)
        stacked_key_matrix = key_now * jnp.exp(-cum_decay)
        stacked_receptance = read_now * jnp.exp(cum_decay)
        m_ab = pair_table(decay_matrix_a, decay_matrix_b, strict)
        m_ak = pair_table(decay_matrix_a, stacked_key_matrix, strict)
        m_rb = pair_table(stacked_receptance, decay_matrix_b, inclusive)
        m_rk = pair_table(stacked_receptance, stacked_key_matrix, inclusive)
        right_operand = jnp.einsum(
            "bvq,bzq->bvz", decay_matrix_a, state_per_block, precision=EXACT_PRECISION
        ) + jnp.einsum("hij,hjm->him", m_ak, current_value, precision=EXACT_PRECISION)
        delta_updates = jnp.einsum(
            "hij,hjm->him", unit_inverse(m_ab), right_operand, precision=EXACT_PRECISION
        )
        block_out = (
            jnp.einsum(
                "bvq,bzq->bvz", stacked_receptance, state_per_block, precision=EXACT_PRECISION
            )
            + jnp.einsum("hij,hjm->him", m_rb, delta_updates, precision=EXACT_PRECISION)
            + jnp.einsum("hij,hjm->him", m_rk, current_value, precision=EXACT_PRECISION)
        )
        grown_state = (
            state_per_block
            + jnp.einsum("sao,sac->soc", delta_updates, decay_matrix_b, precision=EXACT_PRECISION)
            + jnp.einsum(
                "sao,sac->soc", current_value, stacked_key_matrix, precision=EXACT_PRECISION
            )
        )
        return (grown_state * jnp.exp(cum_decay[:, -1])[:, None, :], block_out)

    final_state, block_outs = lax.scan(
        block_step, start_pair, (read_vals, key_vals, removal, writing, decay_vals, stacked)
    )

    def chain(earlier, later_pair):
        moved_state = jnp.einsum(
            "hmk,hkj->hmj", earlier, later_pair[:, :HEAD], precision=EXACT_PRECISION
        )
        return moved_state + jnp.concatenate(
            [jnp.zeros_like(later_pair[:, HEAD:]), later_pair[:, HEAD:]], axis=1
        )

    carried = prefix(final_state, "sp", chain, start_pair)
    incoming = carried[:, HEAD:]
    result = block_outs[..., HEAD:] + jnp.einsum(
        "nhlm,hvm->nhlv", block_outs[..., :HEAD], incoming, precision=EXACT_PRECISION
    )
    mean_val = jnp.mean(result, axis=-1, keepdims=True)
    centered = result - mean_val
    variance = jnp.mean(centered * centered, axis=-1, keepdims=True)
    normed = (
        (centered * lax.rsqrt(variance + GROUP_EPS))
        .transpose(0, 2, 1, 3)
        .reshape(num_rows, num_heads * HEAD)
    )
    return (normed * group_gain).astype(jnp.bfloat16)


def per_device(
    tokens,
    norm_gain,
    query_w,
    key_w,
    value_w,
    recept_w,
    rec_key_w,
    rec_value_w,
    decay_down,
    decay_up,
    decay_base,
    learn_rate,
    query_gain,
    key_gain,
    sink_logit,
    group_gain,
    out_att_w,
    out_rec_w,
):
    groups = lax.axis_size(("fs", "tp"))
    own_width = tokens.shape[1]
    own_values = tokens.astype(jnp.float32)
    squares = lax.psum(jnp.sum(own_values * own_values, axis=1), ("fs", "tp"))
    gain_part = lax.dynamic_slice_in_dim(
        norm_gain, lax.axis_index(("fs", "tp")) * own_width, own_width, 0
    )
    scaled = own_values * lax.rsqrt(squares / (own_width * groups) + NORM_EPS)[:, None] * gain_part
    outgoing = scaled.astype(jnp.bfloat16)
    gathered = lax.all_gather(outgoing, ("fs", "tp"), axis=1, tiled=True)

    def rounded(sums):
        return lax.optimization_barrier(
            tuple((acc_total.astype(jnp.bfloat16) for acc_total in sums))
        )

    rec_span = recept_w.shape[1]
    decay_cols = lax.dynamic_slice_in_dim(
        decay_up, lax.axis_index(("fs", "tp")) * rec_span, rec_span, 1
    )
    decay_low = jnp.tanh(jnp.dot(gathered, decay_down, preferred_element_type=jnp.float32)).astype(
        jnp.bfloat16
    )
    decay_rate = jnp.dot(decay_low, decay_cols, preferred_element_type=jnp.float32) + jnp.repeat(
        decay_base.T, HEAD, axis=1
    )
    log_decay = -jnp.exp(decay_rate)
    pieces = (
        lax.all_gather(query_w, "sp", axis=0, tiled=True),
        lax.all_gather(key_w, "sp", axis=0, tiled=True),
        lax.all_gather(value_w, "sp", axis=0, tiled=True),
        lax.all_gather(recept_w, "sp", axis=0, tiled=True),
        lax.all_gather(rec_key_w, "sp", axis=0, tiled=True),
        lax.all_gather(rec_value_w, "sp", axis=0, tiled=True),
    )
    all_sums = tuple(
        (
            jnp.dot(gathered, weight_piece, preferred_element_type=jnp.float32)
            for weight_piece in pieces
        )
    )
    att_inputs = rounded(all_sums[:3])
    att_mix, row_lse = attend(
        att_inputs[0], att_inputs[1], att_inputs[2], query_gain, key_gain, sink_logit
    )
    rec_sums = all_sums[3:]
    rec_inputs = rounded(rec_sums)
    rec_mix = recur(rec_inputs[0], rec_inputs[1], rec_inputs[2], log_decay, learn_rate, group_gain)
    att_full, rec_full = (
        lax.all_gather(out_att_w, "sp", axis=1, tiled=True),
        lax.all_gather(out_rec_w, "sp", axis=1, tiled=True),
    )
    mixed_out = lax.psum_scatter(
        (
            jnp.dot(att_mix, att_full, preferred_element_type=jnp.float32)
            + jnp.dot(rec_mix, rec_full, preferred_element_type=jnp.float32)
        ).astype(jnp.bfloat16),
        ("fs", "tp"),
        scatter_dimension=0,
        tiled=True,
    )
    return (mixed_out, row_lse)


def solution(mesh):
    in_specs = (
        P("sp", ("fs", "tp")),
        P(),
        P("sp", ("fs", "tp")),
        P("sp", ("fs", "tp")),
        P("sp", ("fs", "tp")),
        P("sp", ("fs", "tp")),
        P("sp", ("fs", "tp")),
        P("sp", ("fs", "tp")),
        P(),
        P(),
        P(("fs", "tp"), "sp"),
        P(("fs", "tp")),
        P(),
        P(),
        P(("fs", "tp")),
        P(("fs", "tp")),
        P(("fs", "tp"), "sp"),
        P(("fs", "tp"), "sp"),
    )
    out_specs = (P(("sp", "fs", "tp"), None), P(("fs", "tp"), "sp"))
    return jax.shard_map(
        per_device, mesh=mesh, in_specs=in_specs, out_specs=out_specs, check_vma=False
    )
```

profile of v0, /device:TPU:0, one launch (start us, length us, event | category | flops | bytes accessed | tf_op | source)
XLA Modules:
  0.0 263.2 jit_solution(7685932151415955385)
XLA Ops:
  7.3 1.1 fusion.33
  8.4 15.2 %psum.7 = f32[256]{0:T(256)S(1)} all-reduce(f32[256]{0:T(256)S(1)} %fusion.33), channel_id=1, replica_groups=mesh['sp'=4,'fs'=4,'tp'=2] {'fs','tp'}, use_global_device_ids=true, to_apply=%region_1.0 | all-reduce | flops 256 | bytes 2048 | tf_op jit(solution)/shard_map/psum | solution.py:216
  23.6 0.8 dynamic_slice.33
  24.3 1.7 fusion.35
  26.1 0.7 mul.191
  26.9 0.7 broadcast_in_dim.98
  27.6 0.8 copy.65
  28.4 16.6 %all_gather.35 = bf16[2048,64]{0,1:T(8,128)(2,1)} all-gather(bf16[512,64]{0,1:T(8,128)(2,1)} %param.25), channel_id=1, replica_groups=mesh['sp'=4,'fs'=4,'tp'=2] {'sp'}, dimensions={0}, use_global_device_ids=true | all-gather | bytes 327680 | tf_op jit(solution)/shard_map/all_gather | solution.py:242
  45.0 15.2 %all_gather.36 = bf16[2048,64]{0,1:T(8,128)(2,1)} all-gather(bf16[512,64]{0,1:T(8,128)(2,1)} %param.26), channel_id=1, replica_groups=mesh['sp'=4,'fs'=4,'tp'=2] {'sp'}, dimensions={0}, use_global_device_ids=true | all-gather | bytes 327680 | tf_op jit(solution)/shard_map/all_gather | solution.py:243
  60.2 15.3 %all_gather.34 = bf16[2048,128]{1,0:T(8,128)(2,1)S(1)} all-gather(bf16[512,128]{1,0:T(8,128)(2,1)S(1)} %copy-done.10), channel_id=1, replica_groups=mesh['sp'=4,'fs'=4,'tp'=2] {'sp'}, dimensions={0}, use_global_device_ids=true | all-gather | bytes 655360 | tf_op jit(solution)/shard_map/all_gather | solution.py:241
  75.5 15.5 %all_gather.38 = bf16[2048,128]{1,0:T(8,128)(2,1)S(1)} all-gather(bf16[512,128]{1,0:T(8,128)(2,1)S(1)} %copy-done.11), channel_id=1, replica_groups=mesh['sp'=4,'fs'=4,'tp'=2] {'sp'}, dimensions={0}, use_global_device_ids=true | all-gather | bytes 655360 | tf_op jit(solution)/shard_map/all_gather | solution.py:244
  91.0 16.3 %all_gather.39 = bf16[2048,128]{1,0:T(8,128)(2,1)S(1)} all-gather(bf16[512,128]{1,0:T(8,128)(2,1)S(1)} %copy-done.12), channel_id=1, replica_groups=mesh['sp'=4,'fs'=4,'tp'=2] {'sp'}, dimensions={0}, use_global_device_ids=true | all-gather | bytes 655360 | tf_op jit(solution)/shard_map/all_gather | solution.py:245
  107.3 15.9 %all_gather.40 = bf16[2048,128]{1,0:T(8,128)(2,1)S(1)} all-gather(bf16[512,128]{1,0:T(8,128)(2,1)S(1)} %copy-done.13), channel_id=1, replica_groups=mesh['sp'=4,'fs'=4,'tp'=2] {'sp'}, dimensions={0}, use_global_device_ids=true | all-gather | bytes 655360 | tf_op jit(solution)/shard_map/all_gather | solution.py:246
  123.2 16.1 %all_gather.37 = bf16[128,2048]{1,0:T(8,128)(2,1)} all-gather(bf16[128,512]{1,0:T(8,128)(2,1)S(1)} %copy-done.14), channel_id=1, replica_groups=mesh['sp'=4,'fs'=4,'tp'=2] {'sp'}, dimensions={1}, use_global_device_ids=true | all-gather | bytes 655360 | tf_op jit(solution)/shard_map/all_gather | solution.py:262
  139.3 15.6 %all_gather.43 = bf16[128,2048]{1,0:T(8,128)(2,1)} all-gather(bf16[128,512]{1,0:T(8,128)(2,1)S(1)} %copy-done.15), channel_id=1, replica_groups=mesh['sp'=4,'fs'=4,'tp'=2] {'sp'}, dimensions={1}, use_global_device_ids=true | all-gather | bytes 655360 | tf_op jit(solution)/shard_map/all_gather | solution.py:263
  155.1 0.8 broadcast_and_fusion
  155.8 1.8 convolution_convert_fusion.6
  157.6 1.7 convolution_convert_fusion.5
  159.3 0.4 convolution_convert_fusion.3
  159.9 0.4 convolution_convert_fusion.2
  160.3 0.4 convolution_convert_fusion.1
  160.8 0.4 convolution_convert_fusion
  161.2 0.2 reshape.254
  161.6 1.4 fusion.29
  163.3 3.1 %collective-permute-start = (bf16[128,128]{0,1:T(8,128)(2,1)S(1)}, bf16[128,128]{0,1:T(8,128)(2,1)S(1)}, u32[]{:S(2)}, u32[]{:S(2)}) collective-permute-start(bf16[128,128]{0,1:T(8,128)(2,1)S(1)} %get-tuple-element.242), channel_id=1, source_target_pairs={{0,8},{8,16},{16,24},{1,9},{9,17},{17,25},{2,10},{10,18},{18,26},{... | collective-permute-start | bytes 98312 | tf_op jit(solution)/shard_map/ppermute | solution.py:19
  166.9 0.2 reshape.255
  167.4 35.9 %while.28 = (s32[]{:T(128)}, f32[2,128,64]{1,2,0:T(8,128)S(1)}, f32[8,2,32,128]{3,2,0,1:T(8,128)}, f32[8,2,32,64]{3,2,1,0:T(8,128)S(1)}, f32[8,2,32,64]{3,2,1,0:...) while((s32[]{:T(128)}, f32[2,128,64]{1,2,0:T(8,128)S(1)}, ...), condition=%wide.region_9.10_spmd.clone.clone, body=%wide.region_7.9_spmd.clone.clone.sunk | while | flops 50579456 | bytes 1623177 | solution.py:165
  170.5 0.3 convolution_add_fusion.23
  170.8 0.3 fusion.229
  171.1 0.8 fusion.232
  175.0 0.3 convolution_add_fusion.23
  175.3 0.3 fusion.229
  175.6 0.8 fusion.232
  179.4 0.3 convolution_add_fusion.23
  179.7 0.3 fusion.229
  180.0 0.8 fusion.232
  183.9 0.3 convolution_add_fusion.23
  184.2 0.3 fusion.229
  184.5 0.8 fusion.232
  188.4 0.3 convolution_add_fusion.23
  188.7 0.3 fusion.229
  189.0 0.8 fusion.232
  192.9 0.3 convolution_add_fusion.23
  193.2 0.3 fusion.229
  193.5 0.8 fusion.232
  197.4 0.3 convolution_add_fusion.23
  197.7 0.3 fusion.229
  198.0 0.8 fusion.232
  201.9 0.3 convolution_add_fusion.23
  202.2 0.3 fusion.229
  202.5 0.8 fusion.232
  203.3 13.7 %all-gather = bf16[8,128,64]{1,2,0:T(8,128)(2,1)S(1)} all-gather(bf16[2,128,64]{1,2,0:T(8,128)(2,1)S(1)} %convert_element_type.103), channel_id=2, replica_groups=mesh['sp'=4,'fs'=4,'tp'=2] {'sp'}, dimensions={0}, use_global_device_ids=true | all-gather | bytes 163840 | tf_op jit(solution)/shard_map/all_gather | solution.py:24
  216.9 1.2 while.27
  218.3 0.5 fusion.59
  218.8 0.3 multiply_reduce_fusion
  219.0 0.2 multiply_bitcast_fusion
  219.5 0.2 copy.72
  219.9 0.3 fusion.58
  220.5 0.3 fusion.30
  220.9 0.5 fusion.44
  221.4 0.2 copy-done.5
  221.6 1.4 fusion.24
  223.0 0.7 fusion.55
  223.7 32.7 %reduce-scatter.2.cloned.1.call-done = bf16[32,2048]{1,0:T(8,128)(2,1)} async-done(((bf16[256,2048]{1,0:T(8,128)(2,1)}), bf16[32,2048]{1,0:T(8,128)(2,1)}) %reduce-scatter.2.cloned.1.call-update) | async-done | bytes 131088 | tf_op jit(solution)/shard_map/reduce_scatter | solution.py:265
  (294 shorter events, 27.3 us)
Async XLA Ops:
  7.2 154.4 %copy-start = (bf16[2048,64]{0,1:T(8,128)(2,1)S(1)}, bf16[2048,64]{0,1:T(8,128)(2,1)}, u32[]{:S(2)}) copy-start(bf16[2048,64]{0,1:T(8,128)(2,1)} %param.30) | copy-start | bytes 786436
  7.2 53.0 %copy-start.10 = (bf16[512,128]{1,0:T(8,128)(2,1)S(1)}, bf16[512,128]{1,0:T(8,128)(2,1)}, u32[]{:S(2)}) copy-start(bf16[512,128]{1,0:T(8,128)(2,1)} %param.24) | copy-start | bytes 393220
  7.2 68.4 %copy-start.11 = (bf16[512,128]{1,0:T(8,128)(2,1)S(1)}, bf16[512,128]{1,0:T(8,128)(2,1)}, u32[]{:S(2)}) copy-start(bf16[512,128]{1,0:T(8,128)(2,1)} %param.27) | copy-start | bytes 393220
  7.2 83.8 %copy-start.12 = (bf16[512,128]{1,0:T(8,128)(2,1)S(1)}, bf16[512,128]{1,0:T(8,128)(2,1)}, u32[]{:S(2)}) copy-start(bf16[512,128]{1,0:T(8,128)(2,1)} %param.28) | copy-start | bytes 393220
  7.2 100.1 %copy-start.13 = (bf16[512,128]{1,0:T(8,128)(2,1)S(1)}, bf16[512,128]{1,0:T(8,128)(2,1)}, u32[]{:S(2)}) copy-start(bf16[512,128]{1,0:T(8,128)(2,1)} %param.29) | copy-start | bytes 393220
  7.2 148.6 %all-gather.3.cloned.1.call-start = ((), (), s32[]{:S(2)}) async-start(), calls=%async_computation.1 | async-start | bytes 1179648 | tf_op jit(solution)/shard_map/all_gather | solution.py:222
  26.0 97.2 %copy-start.14 = (bf16[128,512]{1,0:T(8,128)(2,1)S(1)}, bf16[128,512]{1,0:T(8,128)(2,1)}, u32[]{:S(2)}) copy-start(bf16[128,512]{1,0:T(8,128)(2,1)} %param.38) | copy-start | bytes 393220
  26.0 230.3 %reduce-scatter.2.cloned.1.call-start = ((), (), s32[]{:S(2)}) async-start(), calls=%async_computation.2 | async-start | bytes 1179648 | tf_op jit(solution)/shard_map/reduce_scatter | solution.py:265
  26.9 112.5 %copy-start.2 = (f32[2,128,64]{1,2,0:T(8,128)}, f32[2,128,64]{1,2,0:T(8,128)S(1)}, u32[]{:S(2)}) copy-start(f32[2,128,64]{1,2,0:T(8,128)S(1)} %concatenate.37) | copy-start | bytes 196612
  27.6 111.7 %copy-start.15 = (bf16[128,512]{1,0:T(8,128)(2,1)S(1)}, bf16[128,512]{1,0:T(8,128)(2,1)}, u32[]{:S(2)}) copy-start(bf16[128,512]{1,0:T(8,128)(2,1)} %param.39) | copy-start | bytes 393220
  155.8 3.5 %copy-start.1 = (bf16[256,2048]{1,0:T(8,128)(2,1)S(1)}, bf16[256,2048]{1,0:T(8,128)(2,1)}, u32[]{:S(2)}) copy-start(bf16[256,2048]{1,0:T(8,128)(2,1)} %all-gather.3.cloned.1.call-done) | copy-start | bytes 3145732
  160.3 1.3 copy-start.7
  160.8 2.5 copy-start.17
  163.0 4.4 %copy-start.4 = (f32[2,128,64]{1,2,0:T(8,128)S(1)}, f32[2,128,64]{1,2,0:T(8,128)}, u32[]{:S(2)}) copy-start(f32[2,128,64]{1,2,0:T(8,128)} %copy-done.2) | copy-start | bytes 196612
  163.3 56.5 %collective-permute-start = (bf16[128,128]{0,1:T(8,128)(2,1)S(1)}, bf16[128,128]{0,1:T(8,128)(2,1)S(1)}, u32[]{:S(2)}, u32[]{:S(2)}) collective-permute-start(bf16[128,128]{0,1:T(8,128)(2,1)S(1)} %get-tuple-element.242), channel_id=1, source_target_pairs={{0,8},{8,16},{16,24},{1,9},{9,17},{17,25},{2,10},{10,18},{18,26},{... | collective-permute-start | bytes 98312 | tf_op jit(solution)/shard_map/ppermute | solution.py:19
  167.4 49.6 %copy-start.3 = (f32[2,128,64]{1,2,0:T(8,128)S(1)}, f32[2,128,64]{1,2,0:T(8,128)}, u32[]{:S(2)}) copy-start(f32[2,128,64]{1,2,0:T(8,128)} %copy-done.2) | copy-start | bytes 196612
  203.2 15.0 %copy-start.8 = (f32[8,2,32,128]{3,2,0,1:T(8,128)S(1)}, f32[8,2,32,128]{3,2,0,1:T(8,128)}, u32[]{:S(2)}) copy-start(f32[8,2,32,128]{3,2,0,1:T(8,128)} %get-tuple-element.157) | copy-start | bytes 786436
  203.3 16.0 %copy-start.18 = (f32[64]{0:T(128)S(1)}, f32[64]{0:T(128)}, u32[]{:S(2)}) copy-start(f32[64]{0:T(128)} %param.34) | copy-start | bytes 772
  218.1 1.8 copy-start.9
  218.2 2.1 copy-start.16
  219.9 1.0 copy-start.6
  220.5 1.1 copy-start.5
  220.5 1.1 copy-start.19
Sparse Core Ops, SparseCore 0:
  26.1 22.8 all-gather.2
  223.1 33.1 reduce-scatter.1
where the time goes:
time: 264 us; the launch traced here: 263 us
  blocking collectives  155 us (59%)
  matrix products  43.7 us (17%)
  waiting for transfers between devices  32.7 us (12%)
  between operations  14.6 us (6%)
  other arithmetic  6.77 us (3%)
  local copies, waits for them, and re-layouts  5.52 us (2%)
  starting transfers between devices  3.16 us (1%)
    reduce_scatter x1, waiting for transfers between devices, per_device(): lax.psum_scatter((jnp.dot(att_mix, att_full, preferred_element_type=jnp.f...  32.7 us
    all_gather x1, blocking collectives, per_device(): lax.all_gather(key_w, 'sp', axis=0, tiled=True)  16.6 us
    all_gather x1, blocking collectives, per_device(): lax.all_gather(rec_key_w, 'sp', axis=0, tiled=True)  16.3 us
    all_gather x1, blocking collectives, per_device(): lax.all_gather(out_att_w, 'sp', axis=1, tiled=True)  16.1 us
    all_gather x1, blocking collectives, per_device(): lax.all_gather(rec_value_w, 'sp', axis=0, tiled=True)  15.9 us
    all_gather x1, blocking collectives, per_device(): lax.all_gather(out_rec_w, 'sp', axis=1, tiled=True)  15.6 us
    all_gather x1, blocking collectives, per_device(): lax.all_gather(recept_w, 'sp', axis=0, tiled=True)  15.5 us
    all_gather x1, blocking collectives, per_device(): lax.all_gather(query_w, 'sp', axis=0, tiled=True)  15.3 us
  transfers between devices with their start and end apart: 3, of which 1 were waited for; matrix products, arithmetic and copies ran while one was open for 16% of the time, Pallas kernels for 0%

commit v1 on v0

--- a/solution.py
+++ b/solution.py
@@ -213,7 +213,7 @@
     groups = lax.axis_size(("fs", "tp"))
     own_width = tokens.shape[1]
     own_values = tokens.astype(jnp.float32)
-    squares = lax.psum(jnp.sum(own_values * own_values, axis=1), ("fs", "tp"))
+    squares = lax.psum(lax.psum(jnp.sum(own_values * own_values, axis=1), "fs"), "tp")
     gain_part = lax.dynamic_slice_in_dim(
         norm_gain, lax.axis_index(("fs", "tp")) * own_width, own_width, 0
     )

time: 264 us -> 263 us (level)
    psum x1 -> x2, blocking collectives: 15.2 us -> 13.8 us  [the longest x1 11.4 us: per_device(): lax.psum(jnp.sum(own_values * own_values, axis=1), 'fs')]
where the time goes in v1:
time: 263 us; the launch traced here: 262 us
  blocking collectives  153 us (58%)
  matrix products  43.7 us (17%)
  waiting for transfers between devices  33.9 us (13%)
  between operations  14.6 us (6%)
  other arithmetic  6.78 us (3%)
  local copies, waits for them, and re-layouts  5.51 us (2%)
  starting transfers between devices  3.96 us (2%)
    reduce_scatter x1, waiting for transfers between devices, per_device(): lax.psum_scatter((jnp.dot(att_mix, att_full, preferred_element_type=jnp.f...  33.9 us
    all_gather x1, blocking collectives, per_device(): lax.all_gather(key_w, 'sp', axis=0, tiled=True)  16.2 us
    all_gather x1, blocking collectives, per_device(): lax.all_gather(rec_key_w, 'sp', axis=0, tiled=True)  16.1 us
    all_gather x1, blocking collectives, per_device(): lax.all_gather(out_rec_w, 'sp', axis=1, tiled=True)  15.8 us
    all_gather x1, blocking collectives, per_device(): lax.all_gather(query_w, 'sp', axis=0, tiled=True)  15.7 us
    all_gather x1, blocking collectives, per_device(): lax.all_gather(recept_w, 'sp', axis=0, tiled=True)  15.7 us
    all_gather x1, blocking collectives, per_device(): lax.all_gather(out_att_w, 'sp', axis=1, tiled=True)  15.5 us
    all_gather x1, blocking collectives, per_device(): lax.all_gather(value_w, 'sp', axis=0, tiled=True)  15.4 us
  transfers between devices with their start and end apart: 3, of which 1 were waited for; matrix products, arithmetic and copies ran while one was open for 16% of the time, Pallas kernels for 0%

profile of v1, /device:TPU:0, one launch (start us, length us, event | category | flops | bytes accessed | tf_op | source)
XLA Modules:
  0.0 262.4 jit_solution(3848021720956799064)
XLA Ops:
  7.3 1.1 fusion.33
  8.4 11.4 %psum.14 = f32[256]{0:T(256)S(1)} all-reduce(f32[256]{0:T(256)S(1)} %fusion.33), channel_id=1, replica_groups=mesh['sp'=4,'fs'=4,'tp'=2] {'fs'}, use_global_device_ids=true, to_apply=%region_1.0 | all-reduce | flops 256 | bytes 2048 | tf_op jit(solution)/shard_map/psum | solution.py:216
  19.8 2.5 psum.15
  22.3 0.8 dynamic_slice.33
  23.0 1.7 fusion.35
  24.8 0.7 mul.191
  25.6 0.7 broadcast_in_dim.98
  26.3 0.7 copy.65
  27.1 16.2 %all_gather.35 = bf16[2048,64]{0,1:T(8,128)(2,1)} all-gather(bf16[512,64]{0,1:T(8,128)(2,1)} %param.25), channel_id=1, replica_groups=mesh['sp'=4,'fs'=4,'tp'=2] {'sp'}, dimensions={0}, use_global_device_ids=true | all-gather | bytes 327680 | tf_op jit(solution)/shard_map/all_gather | solution.py:242
  43.3 15.4 %all_gather.36 = bf16[2048,64]{0,1:T(8,128)(2,1)} all-gather(bf16[512,64]{0,1:T(8,128)(2,1)} %param.26), channel_id=1, replica_groups=mesh['sp'=4,'fs'=4,'tp'=2] {'sp'}, dimensions={0}, use_global_device_ids=true | all-gather | bytes 327680 | tf_op jit(solution)/shard_map/all_gather | solution.py:243
  58.7 15.7 %all_gather.34 = bf16[2048,128]{1,0:T(8,128)(2,1)S(1)} all-gather(bf16[512,128]{1,0:T(8,128)(2,1)S(1)} %copy-done.10), channel_id=1, replica_groups=mesh['sp'=4,'fs'=4,'tp'=2] {'sp'}, dimensions={0}, use_global_device_ids=true | all-gather | bytes 655360 | tf_op jit(solution)/shard_map/all_gather | solution.py:241
  74.3 15.7 %all_gather.38 = bf16[2048,128]{1,0:T(8,128)(2,1)S(1)} all-gather(bf16[512,128]{1,0:T(8,128)(2,1)S(1)} %copy-done.11), channel_id=1, replica_groups=mesh['sp'=4,'fs'=4,'tp'=2] {'sp'}, dimensions={0}, use_global_device_ids=true | all-gather | bytes 655360 | tf_op jit(solution)/shard_map/all_gather | solution.py:244
  90.0 16.1 %all_gather.39 = bf16[2048,128]{1,0:T(8,128)(2,1)S(1)} all-gather(bf16[512,128]{1,0:T(8,128)(2,1)S(1)} %copy-done.12), channel_id=1, replica_groups=mesh['sp'=4,'fs'=4,'tp'=2] {'sp'}, dimensions={0}, use_global_device_ids=true | all-gather | bytes 655360 | tf_op jit(solution)/shard_map/all_gather | solution.py:245
  106.1 14.7 %all_gather.40 = bf16[2048,128]{1,0:T(8,128)(2,1)S(1)} all-gather(bf16[512,128]{1,0:T(8,128)(2,1)S(1)} %copy-done.13), channel_id=1, replica_groups=mesh['sp'=4,'fs'=4,'tp'=2] {'sp'}, dimensions={0}, use_global_device_ids=true | all-gather | bytes 655360 | tf_op jit(solution)/shard_map/all_gather | solution.py:246
  120.8 15.5 %all_gather.37 = bf16[128,2048]{1,0:T(8,128)(2,1)} all-gather(bf16[128,512]{1,0:T(8,128)(2,1)S(1)} %copy-done.14), channel_id=1, replica_groups=mesh['sp'=4,'fs'=4,'tp'=2] {'sp'}, dimensions={1}, use_global_device_ids=true | all-gather | bytes 655360 | tf_op jit(solution)/shard_map/all_gather | solution.py:262
  136.3 15.8 %all_gather.43 = bf16[128,2048]{1,0:T(8,128)(2,1)} all-gather(bf16[128,512]{1,0:T(8,128)(2,1)S(1)} %copy-done.15), channel_id=1, replica_groups=mesh['sp'=4,'fs'=4,'tp'=2] {'sp'}, dimensions={1}, use_global_device_ids=true | all-gather | bytes 655360 | tf_op jit(solution)/shard_map/all_gather | solution.py:263
  152.2 0.8 broadcast_and_fusion
  153.0 1.8 convolution_convert_fusion.6
  154.8 1.7 convolution_convert_fusion.5
  156.5 0.4 convolution_convert_fusion.3
  157.1 0.4 convolution_convert_fusion.2
  157.5 0.4 convolution_convert_fusion.1
  157.9 0.4 convolution_convert_fusion
  158.4 0.2 reshape.254
  158.8 1.4 fusion.29
  160.5 3.9 %collective-permute-start = (bf16[128,128]{0,1:T(8,128)(2,1)S(1)}, bf16[128,128]{0,1:T(8,128)(2,1)S(1)}, u32[]{:S(2)}, u32[]{:S(2)}) collective-permute-start(bf16[128,128]{0,1:T(8,128)(2,1)S(1)} %get-tuple-element.242), channel_id=1, source_target_pairs={{0,8},{8,16},{16,24},{1,9},{9,17},{17,25},{2,10},{10,18},{18,26},{... | collective-permute-start | bytes 98312 | tf_op jit(solution)/shard_map/ppermute | solution.py:19
  165.3 35.9 %while.28 = (s32[]{:T(128)}, f32[2,128,64]{1,2,0:T(8,128)S(1)}, f32[8,2,32,128]{3,2,0,1:T(8,128)}, f32[8,2,32,64]{3,2,1,0:T(8,128)S(1)}, f32[8,2,32,64]{3,2,1,0:...) while((s32[]{:T(128)}, f32[2,128,64]{1,2,0:T(8,128)S(1)}, ...), condition=%wide.region_10.11_spmd.clone.clone, body=%wide.region_8.10_spmd.clone.clone.sunk | while | flops 50579456 | bytes 1623177 | solution.py:165
  168.5 0.3 convolution_add_fusion.23
  168.8 0.3 fusion.229
  169.1 0.8 fusion.232
  172.9 0.3 convolution_add_fusion.23
  173.2 0.3 fusion.229
  173.5 0.8 fusion.232
  177.4 0.3 convolution_add_fusion.23
  177.7 0.3 fusion.229
  178.0 0.8 fusion.232
  181.9 0.3 convolution_add_fusion.23
  182.2 0.3 fusion.229
  182.5 0.8 fusion.232
  186.4 0.3 convolution_add_fusion.23
  186.7 0.3 fusion.229
  187.0 0.8 fusion.232
  190.8 0.3 convolution_add_fusion.23
  191.1 0.3 fusion.229
  191.4 0.8 fusion.232
  195.3 0.3 convolution_add_fusion.23
  195.6 0.3 fusion.229
  195.9 0.8 fusion.232
  199.8 0.3 convolution_add_fusion.23
  200.1 0.3 fusion.229
  200.4 0.8 fusion.232
  201.2 13.6 %all-gather = bf16[8,128,64]{1,2,0:T(8,128)(2,1)S(1)} all-gather(bf16[2,128,64]{1,2,0:T(8,128)(2,1)S(1)} %convert_element_type.103), channel_id=2, replica_groups=mesh['sp'=4,'fs'=4,'tp'=2] {'sp'}, dimensions={0}, use_global_device_ids=true | all-gather | bytes 163840 | tf_op jit(solution)/shard_map/all_gather | solution.py:24
  214.9 1.2 while.27
  216.2 0.5 fusion.59
  216.7 0.3 multiply_reduce_fusion
  217.0 0.2 multiply_bitcast_fusion
  217.4 0.2 copy.72
  217.9 0.3 fusion.58
  218.5 0.3 fusion.30
  218.9 0.5 fusion.44
  219.3 0.2 copy-done.5
  219.5 1.4 fusion.24
  221.0 0.7 fusion.55
  221.6 33.9 %reduce-scatter.2.cloned.1.call-done = bf16[32,2048]{1,0:T(8,128)(2,1)} async-done(((bf16[256,2048]{1,0:T(8,128)(2,1)}), bf16[32,2048]{1,0:T(8,128)(2,1)}) %reduce-scatter.2.cloned.1.call-update) | async-done | bytes 131088 | tf_op jit(solution)/shard_map/reduce_scatter | solution.py:265
  (295 shorter events, 27.5 us)
Async XLA Ops:
  7.2 151.6 %copy-start = (bf16[2048,64]{0,1:T(8,128)(2,1)S(1)}, bf16[2048,64]{0,1:T(8,128)(2,1)}, u32[]{:S(2)}) copy-start(bf16[2048,64]{0,1:T(8,128)(2,1)} %param.30) | copy-start | bytes 786436
  7.2 51.5 %copy-start.10 = (bf16[512,128]{1,0:T(8,128)(2,1)S(1)}, bf16[512,128]{1,0:T(8,128)(2,1)}, u32[]{:S(2)}) copy-start(bf16[512,128]{1,0:T(8,128)(2,1)} %param.24) | copy-start | bytes 393220
  7.2 67.1 %copy-start.11 = (bf16[512,128]{1,0:T(8,128)(2,1)S(1)}, bf16[512,128]{1,0:T(8,128)(2,1)}, u32[]{:S(2)}) copy-start(bf16[512,128]{1,0:T(8,128)(2,1)} %param.27) | copy-start | bytes 393220
  7.2 82.8 %copy-start.12 = (bf16[512,128]{1,0:T(8,128)(2,1)S(1)}, bf16[512,128]{1,0:T(8,128)(2,1)}, u32[]{:S(2)}) copy-start(bf16[512,128]{1,0:T(8,128)(2,1)} %param.28) | copy-start | bytes 393220
  7.2 98.9 %copy-start.13 = (bf16[512,128]{1,0:T(8,128)(2,1)S(1)}, bf16[512,128]{1,0:T(8,128)(2,1)}, u32[]{:S(2)}) copy-start(bf16[512,128]{1,0:T(8,128)(2,1)} %param.29) | copy-start | bytes 393220
  7.2 145.8 %all-gather.3.cloned.1.call-start = ((), (), s32[]{:S(2)}) async-start(), calls=%async_computation.1 | async-start | bytes 1179648 | tf_op jit(solution)/shard_map/all_gather | solution.py:222
  24.7 96.1 %copy-start.14 = (bf16[128,512]{1,0:T(8,128)(2,1)S(1)}, bf16[128,512]{1,0:T(8,128)(2,1)}, u32[]{:S(2)}) copy-start(bf16[128,512]{1,0:T(8,128)(2,1)} %param.38) | copy-start | bytes 393220
  24.7 230.8 %reduce-scatter.2.cloned.1.call-start = ((), (), s32[]{:S(2)}) async-start(), calls=%async_computation.2 | async-start | bytes 1179648 | tf_op jit(solution)/shard_map/reduce_scatter | solution.py:265
  25.6 110.7 %copy-start.2 = (f32[2,128,64]{1,2,0:T(8,128)}, f32[2,128,64]{1,2,0:T(8,128)S(1)}, u32[]{:S(2)}) copy-start(f32[2,128,64]{1,2,0:T(8,128)S(1)} %concatenate.37) | copy-start | bytes 196612
  26.3 110.0 %copy-start.15 = (bf16[128,512]{1,0:T(8,128)(2,1)S(1)}, bf16[128,512]{1,0:T(8,128)(2,1)}, u32[]{:S(2)}) copy-start(bf16[128,512]{1,0:T(8,128)(2,1)} %param.39) | copy-start | bytes 393220
  153.0 3.5 %copy-start.1 = (bf16[256,2048]{1,0:T(8,128)(2,1)S(1)}, bf16[256,2048]{1,0:T(8,128)(2,1)}, u32[]{:S(2)}) copy-start(bf16[256,2048]{1,0:T(8,128)(2,1)} %all-gather.3.cloned.1.call-done) | copy-start | bytes 3145732
  157.5 1.3 copy-start.7
  157.9 2.5 copy-start.17
  160.2 5.2 %copy-start.4 = (f32[2,128,64]{1,2,0:T(8,128)S(1)}, f32[2,128,64]{1,2,0:T(8,128)}, u32[]{:S(2)}) copy-start(f32[2,128,64]{1,2,0:T(8,128)} %copy-done.2) | copy-start | bytes 196612
  160.5 57.3 %collective-permute-start = (bf16[128,128]{0,1:T(8,128)(2,1)S(1)}, bf16[128,128]{0,1:T(8,128)(2,1)S(1)}, u32[]{:S(2)}, u32[]{:S(2)}) collective-permute-start(bf16[128,128]{0,1:T(8,128)(2,1)S(1)} %get-tuple-element.242), channel_id=1, source_target_pairs={{0,8},{8,16},{16,24},{1,9},{9,17},{17,25},{2,10},{10,18},{18,26},{... | collective-permute-start | bytes 98312 | tf_op jit(solution)/shard_map/ppermute | solution.py:19
  165.3 49.5 %copy-start.3 = (f32[2,128,64]{1,2,0:T(8,128)S(1)}, f32[2,128,64]{1,2,0:T(8,128)}, u32[]{:S(2)}) copy-start(f32[2,128,64]{1,2,0:T(8,128)} %copy-done.2) | copy-start | bytes 196612
  201.2 15.0 %copy-start.8 = (f32[8,2,32,128]{3,2,0,1:T(8,128)S(1)}, f32[8,2,32,128]{3,2,0,1:T(8,128)}, u32[]{:S(2)}) copy-start(f32[8,2,32,128]{3,2,0,1:T(8,128)} %get-tuple-element.157) | copy-start | bytes 786436
  201.2 16.0 %copy-start.18 = (f32[64]{0:T(128)S(1)}, f32[64]{0:T(128)}, u32[]{:S(2)}) copy-start(f32[64]{0:T(128)} %param.34) | copy-start | bytes 772
  216.1 1.8 copy-start.9
  216.1 2.1 copy-start.16
  217.8 1.0 copy-start.6
  218.5 1.1 copy-start.5
  218.5 1.1 copy-start.19
Sparse Core Ops, SparseCore 0:
  24.8 22.8 all-gather.2
  221.1 34.4 reduce-scatter.1
